TPU v7x, 32 devices: a whole 2x2x4 slice. The times are simulated.
32 devices in a mesh: ep: 8 (over z, core), tp: 4 (over y, x).
Axes of the slice: x: 2, y: 2, z: 4, core: 2. Of those that a mesh axis runs over, the one named last changes fastest.
Arguments:
- tokens: bfloat16 [128, 2048], P('ep'), may hold values from -6 to 6
- attn_gain: float32 [2048], replicated, may hold values from 0.1 to 1.9
- query_weight: bfloat16 [2048, 2048], P('ep', 'tp'), may hold values from -0.125 to 0.125
- key_weight: bfloat16 [2048, 2048], P('ep', 'tp'), may hold values from -0.125 to 0.125
- value_weight: bfloat16 [2048, 2048], P('ep', 'tp'), may hold values from -0.125 to 0.125
- forget_weight: bfloat16 [2048, 16], P(None, 'tp'), may hold values from -0.125 to 0.125
- forget_bias: float32 [16], P('tp'), may hold values from -1 to 2
- cache_keys: bfloat16 [128, 16, 384, 128], P('ep', 'tp'), may hold values from -240 to 240
- cache_values: bfloat16 [128, 16, 384, 128], P('ep', 'tp'), may hold values from -6 to 6
- cache_gates: float32 [128, 16, 384], P('ep', 'tp'), may hold values from -768 to 0, as said below
- lengths: int32 [128], P('ep'), may hold values from 1 to 384
- output_weight: bfloat16 [2048, 2048], P('tp', 'ep'), may hold values from -0.125 to 0.125
- ffn_gain: float32 [2048], replicated, may hold values from 0.1 to 1.9
- dense_gate_proj: bfloat16 [2048, 2048], P('ep', 'tp'), may hold values from -0.125 to 0.125
- dense_up_proj: bfloat16 [2048, 2048], P('ep', 'tp'), may hold values from -0.125 to 0.125
- dense_down_proj: bfloat16 [2048, 2048], P('tp', 'ep'), may hold values from -0.125 to 0.125
- dense_mix: bfloat16 [2048], replicated, may hold values from -0.125 to 0.125
- expert_ids: int32 [128, 2], P('ep'), may hold values from 0 to 7, as said below
- group_prob: float32 [128], P('ep'), may hold values from 0.25 to 1
- pair_prob: float32 [128, 2], P('ep'), may hold values from 0.05 to 1
- expert_gate: bfloat16 [8, 2048, 2048], P('ep', None, 'tp'), may hold values from -0.125 to 0.125
- expert_up: bfloat16 [8, 2048, 2048], P('ep', None, 'tp'), may hold values from -0.125 to 0.125
- expert_down: bfloat16 [8, 2048, 2048], P('ep', 'tp'), may hold values from -0.125 to 0.125
Outputs:
- mixed_out: bfloat16 [128, 2048], P('ep')
Inputs may be any that keep to these rules, and one draw needn't show every extreme that they name: `expert_ids`: each row names two different experts of one group, the groups being 4 runs of consecutive ids. In each aligned block of 16 rows (the rows of one index of ep) no expert is named more than 8 times, and some expert exactly 8 times. `cache_gates`: along positions the values never rise.
All inputs are finite; a program needn't handle non-finite values.
Results may differ from a plain program's by a relative error of at most 0.014.
Values may be sent and summed in bfloat16 or wider, within the bound.
A program may use at most 64 MiB of HBM per device.

v0:
```python
import math
import jax
import jax.numpy as jnp
from jax import lax
from jax.sharding import PartitionSpec as P

EPSILON = 1e-06


def rms_scale(values, norm_gain):
    widened = values.astype(jnp.float32)
    return (
        widened
        * lax.rsqrt(jnp.mean(widened * widened, axis=-1, keepdims=True) + EPSILON)
        * norm_gain
    )


def attend(queries, keys_new, values_new, key_cache, value_cache, gate_cache, lengths, log_forget):
    cache_span = key_cache.shape[2]
    score_scale = 1.0 / math.sqrt(key_cache.shape[3])
    positions = jnp.arange(cache_span, dtype=jnp.int32)
    live_mask = positions[None, :] < lengths[:, None]
    last_mask = positions[None, :] == lengths[:, None] - 1
    last_gate = jnp.sum(jnp.where(last_mask[:, None, :], gate_cache, 0.0), axis=-1)
    gate_now = last_gate + log_forget
    scores = (
        jnp.einsum("shd,shpd->shp", queries, key_cache, preferred_element_type=jnp.float32)
        * score_scale
    )
    scores = scores + gate_now[:, :, None] - gate_cache
    scores = jnp.where(live_mask[:, None, :], scores, -jnp.inf)
    own_score = (
        jnp.sum(queries.astype(jnp.float32) * keys_new.astype(jnp.float32), axis=-1) * score_scale
    )
    row_top = jnp.maximum(jnp.max(scores, axis=-1), own_score)
    raised = jnp.exp(scores - row_top[:, :, None])
    own_raised = jnp.exp(own_score - row_top)
    totals = jnp.sum(raised, axis=-1) + own_raised
    weights_low = (raised / totals[:, :, None]).astype(jnp.bfloat16)
    own_prob = (own_raised / totals).astype(jnp.bfloat16)
    attended = jnp.einsum(
        "shp,shpd->shd", weights_low, value_cache, preferred_element_type=jnp.float32
    )
    attended = attended + own_prob.astype(jnp.float32)[:, :, None] * values_new.astype(jnp.float32)
    return attended.astype(jnp.bfloat16)


def row_term(spread, joined):
    return jnp.dot(spread, joined, preferred_element_type=jnp.float32)


def right_product(left_rows, weight_piece):
    return jnp.dot(left_rows, weight_piece, preferred_element_type=jnp.float32)


def shards(
    tokens,
    attn_gain,
    query_weight,
    key_weight,
    value_weight,
    forget_weight,
    forget_bias,
    cache_keys,
    cache_values,
    cache_gates,
    lengths,
    output_weight,
    ffn_gain,
    dense_gate_proj,
    dense_up_proj,
    dense_down_proj,
    dense_mix,
    expert_ids,
    group_prob,
    pair_prob,
    expert_gate,
    expert_up,
    expert_down,
):
    seq_count = tokens.shape[0]
    head_count = cache_keys.shape[1]
    head_size = cache_keys.shape[3]
    proj_width = query_weight.shape[1]
    normed = rms_scale(tokens, attn_gain).astype(jnp.bfloat16)
    spread = lax.all_to_all(normed, "ep", split_axis=1, concat_axis=0, tiled=True)
    joined = jnp.concatenate([query_weight, key_weight, value_weight], axis=1)
    summed = lax.psum_scatter(row_term(spread, joined), "ep", scatter_dimension=0, tiled=True)
    projected = (
        summed[:, :proj_width],
        summed[:, proj_width : 2 * proj_width],
        summed[:, 2 * proj_width :],
    )
    queries = projected[0].astype(jnp.bfloat16).reshape(seq_count, head_count, head_size)
    keys_new = projected[1].astype(jnp.bfloat16).reshape(seq_count, head_count, head_size)
    values_new = projected[2].astype(jnp.bfloat16).reshape(seq_count, head_count, head_size)
    log_forget = jax.nn.log_sigmoid(
        jnp.dot(normed, forget_weight, preferred_element_type=jnp.float32) + forget_bias
    )
    attended = attend(
        queries, keys_new, values_new, cache_keys, cache_values, cache_gates, lengths, log_forget
    )
    attended = attended.reshape(seq_count, head_count * head_size)
    head_terms = right_product(attended, lax.all_gather(output_weight, "ep", axis=1, tiled=True))
    mixed_heads = lax.psum(head_terms, "tp")
    residual = (tokens.astype(jnp.float32) + mixed_heads).astype(jnp.bfloat16)
    ffn_in = rms_scale(residual, ffn_gain).astype(jnp.bfloat16)
    dense_width = dense_gate_proj.shape[1]
    ffn_spread = lax.all_to_all(ffn_in, "ep", split_axis=1, concat_axis=0, tiled=True)
    dense_joined = jnp.concatenate([dense_gate_proj, dense_up_proj], axis=1)
    dense_summed = lax.psum_scatter(
        row_term(ffn_spread, dense_joined).astype(jnp.bfloat16),
        "ep",
        scatter_dimension=0,
        tiled=True,
    ).astype(jnp.float32)
    dense_parts = (dense_summed[:, :dense_width], dense_summed[:, dense_width:])
    dense_hidden = (jax.nn.silu(dense_parts[0]) * dense_parts[1]).astype(jnp.bfloat16)
    dense_terms = right_product(
        dense_hidden, lax.all_gather(dense_down_proj, "ep", axis=1, tiled=True)
    )
    dense_total = lax.psum(dense_terms.astype(jnp.bfloat16), "tp").astype(jnp.float32)
    mix = jax.nn.sigmoid(jnp.dot(ffn_in, dense_mix, preferred_element_type=jnp.float32))
    expert_count = lax.axis_size("ep") * expert_gate.shape[0]
    capacity = 4 * seq_count // expert_count
    slot_total = expert_count * capacity
    picks = expert_ids.reshape(-1)
    expert_grid = jnp.arange(expert_count, dtype=jnp.int32)
    pick_onehot = (picks[:, None] == expert_grid[None, :]).astype(jnp.int32)
    earlier = jnp.cumsum(pick_onehot, axis=0) - pick_onehot
    slot_rank = jnp.sum(earlier * pick_onehot, axis=1)
    destination = (picks * capacity + slot_rank).reshape(seq_count, 2)
    slot_grid = jnp.arange(slot_total, dtype=jnp.int32)
    select_first = (destination[:, 0:1] == slot_grid[None, :]).astype(jnp.bfloat16)
    select_second = (destination[:, 1:2] == slot_grid[None, :]).astype(jnp.bfloat16)
    selector = select_first + select_second
    outbound = jnp.einsum("sk,sd->kd", selector, ffn_in, preferred_element_type=jnp.float32)
    outbound = outbound.astype(jnp.bfloat16).reshape(expert_count, capacity, ffn_in.shape[1])
    arrived = lax.all_to_all(outbound, "ep", split_axis=0, concat_axis=0, tiled=True)
    sources, slots_now, feature = arrived.shape
    row_data = arrived.reshape(sources * slots_now, feature)
    gate_part = jnp.dot(row_data, expert_gate[0], preferred_element_type=jnp.float32)
    up_part = jnp.dot(row_data, expert_up[0], preferred_element_type=jnp.float32)
    expert_hidden = (jax.nn.silu(gate_part) * up_part).astype(jnp.bfloat16)
    partial_out = jnp.dot(expert_hidden, expert_down[0], preferred_element_type=jnp.float32)
    expert_result = lax.psum(partial_out.astype(jnp.bfloat16), "tp").astype(jnp.float32)
    returned = lax.all_to_all(
        expert_result.reshape(sources, slots_now, feature).astype(jnp.bfloat16),
        "ep",
        split_axis=0,
        concat_axis=0,
        tiled=True,
    ).astype(jnp.float32)
    returned = returned.reshape(slot_total, ffn_in.shape[1])
    routes = group_prob[:, None] * pair_prob / jnp.sum(pair_prob, axis=1, keepdims=True)
    first_back = returned[destination[:, 0]]
    second_back = returned[destination[:, 1]]
    side_total = (
        routes[:, 0:1] * first_back + routes[:, 1:2] * second_back + mix[:, None] * dense_total
    )
    result = residual.astype(jnp.float32) + side_total
    return result.astype(jnp.bfloat16)


def solution(mesh):
    return jax.shard_map(
        shards,
        mesh=mesh,
        in_specs=(
            P("ep", None),
            P(),
            P("ep", "tp"),
            P("ep", "tp"),
            P("ep", "tp"),
            P(None, "tp"),
            P("tp"),
            P("ep", "tp", None, None),
            P("ep", "tp", None, None),
            P("ep", "tp", None),
            P("ep"),
            P("tp", "ep"),
            P(),
            P("ep", "tp"),
            P("ep", "tp"),
            P("tp", "ep"),
            P(),
            P("ep", None),
            P("ep"),
            P("ep", None),
            P("ep", None, "tp"),
            P("ep", None, "tp"),
            P("ep", "tp", None),
        ),
        out_specs=P("ep", None),
        check_vma=False,
    )
```

profile of v0, /device:TPU:0, one launch (start us, length us, event | category | flops | bytes accessed | tf_op | source)
XLA Modules:
  0.0 268.5 jit_solution(17298867801017753038)
XLA Ops:
  6.6 1.1 fusion.32
  7.7 0.9 fusion.34
  8.7 12.1 %all_to_all.48 = bf16[16,8,256]{2,0,1:T(8,128)(2,1)S(1)} all-to-all(bf16[16,8,256]{2,0,1:T(8,128)(2,1)S(1)} %bitcast.96), channel_id=1, replica_groups=mesh['ep'=8,'tp'=4] {'ep'}, dimensions={1} | all-to-all | bytes 131072 | tf_op jit(solution)/shard_map/all_to_all | solution.py:87
  20.7 2.3 fusion.20
  24.4 29.2 %reduce-scatter.3.cloned.1.call-done = f32[16,1536]{1,0:T(8,128)} async-done(((f32[128,1536]{1,0:T(8,128)}), f32[16,1536]{1,0:T(8,128)}) %reduce-scatter.3.cloned.1.call-update) | async-done | bytes 98320 | tf_op jit(solution)/shard_map/reduce_scatter | solution.py:89
  53.6 0.9 convert.8
  54.7 5.2 %fusion.80 = f32[16,4,1,384]{3,2,1,0:T(1,128)S(1)} fusion(bf16[16,4,128,1]{2,3,1,0:T(2,128)(2,1)S(1)} %reshape.151, bf16[16,4,384,128]{3,2,1,0:T(8,128)(2,1)} %param.30), kind=kOutput, calls=%fused_computation.117 | convolution fusion | flops 6291456 | bytes 6406144 | tf_op jit(solution)/shard_map/shd,shpd->shp/dot_general | solution.py:28
  60.5 1.2 fusion.48
  61.8 22.4 %all-gather.3.cloned.1.call-done = bf16[512,2048]{1,0:T(8,128)(2,1)} async-done(((bf16[512,256]{1,0:T(8,128)(2,1)}), bf16[512,2048]{1,0:T(8,128)(2,1)}) %all-gather.3.cloned.1.call-update) | async-done | bytes 2097168 | tf_op jit(solution)/shard_map/all_gather | solution.py:105
  84.2 2.6 fusion.55
  86.9 41.4 %all-reduce.4.cloned.1.call-done = f32[16,2048]{1,0:T(8,128)} async-done(((f32[16,2048]{1,0:T(8,128)}), f32[16,2048]{1,0:T(8,128)}) %all-reduce.4.cloned.1.call-update) | async-done | bytes 131088 | tf_op jit(solution)/shard_map/psum | solution.py:106
  128.3 1.0 fusion.36
  129.5 10.3 %all_to_all.49 = bf16[16,8,256]{2,0,1:T(8,128)(2,1)S(1)} all-to-all(bf16[16,8,256]{2,0,1:T(8,128)(2,1)S(1)} %bitcast.97), channel_id=1, replica_groups=mesh['ep'=8,'tp'=4] {'ep'}, dimensions={1} | all-to-all | bytes 131072 | tf_op jit(solution)/shard_map/all_to_all | solution.py:110
  139.8 0.9 convolution_convert_fusion.3
  142.4 12.7 %all_to_all.50 = bf16[8,8,2048]{2,1,0:T(8,128)(2,1)S(1)} all-to-all(bf16[8,8,2048]{2,1,0:T(8,128)(2,1)S(1)} %fusion), channel_id=1, replica_groups=mesh['ep'=8,'tp'=4] {'ep'}, dimensions={0} | all-to-all | bytes 524288 | tf_op jit(solution)/shard_map/all_to_all | solution.py:140
  155.1 2.1 fusion.5
  157.2 3.2 %fusion.1 = bf16[8,8,2048]{2,1,0:T(8,128)(2,1)} fusion(bf16[1,512,2048]{2,1,0:T(8,128)(2,1)S(1)} %copy-done, bf16[1,2048,512]{2,1,0:T(8,128)(2,1)} %param.44, bf16[8,8,2048]{2,1,0:T(8,128)(2,1)S(1)} %all_to_all.50, f32[64,512]{1,0:T(8,128)S(1)} %fusion.5), kind=kOutput, calls=%fused_computation.5 | convolution fusion | flops 268763136 | bytes 4849664 | tf_op jit(solution)/shard_map/dot_general | solution.py:146
  160.5 9.1 %reduce-scatter.5.cloned.1.call-done = bf16[16,1024]{1,0:T(8,128)(2,1)} async-done(((bf16[128,1024]{1,0:T(8,128)(2,1)}), bf16[16,1024]{1,0:T(8,128)(2,1)}) %reduce-scatter.5.cloned.1.call-update) | async-done | bytes 32784 | tf_op jit(solution)/shard_map/reduce_scatter | solution.py:112
  169.6 0.8 convert_element_type.119
  170.3 29.4 %all-gather.5.cloned.1.call-done = bf16[512,2048]{1,0:T(8,128)(2,1)} async-done(((bf16[512,256]{1,0:T(8,128)(2,1)}), bf16[512,2048]{1,0:T(8,128)(2,1)}) %all-gather.5.cloned.1.call-update) | async-done | bytes 2097168 | tf_op jit(solution)/shard_map/all_gather | solution.py:121
  199.7 2.6 convolution_convert_fusion.2
  202.4 42.8 %all-reduce.6.cloned.1.call-done = (bf16[16,2048]{1,0:T(8,128)(2,1)}, bf16[8,8,2048]{2,1,0:T(8,128)(2,1)}) async-done(((bf16[16,2048]{1,0:T(8,128)(2,1)}, bf16[8,8,2048]{2,1,0:T(8,128)(2,1)}), (bf16[16,2048]{1,0:T(8,128)(2,1)}, bf16[8,8,2048]{2,1,0:T(8,128)(2,1)})) %all-reduce.6.cloned.1.call-update) | async-done | bytes 327696 | tf_op jit(solution)/shard_map/psum | solution.py:123
  245.2 4.7 %all-to-all-start.2 = ((bf16[8,8,2048]{2,1,0:T(8,128)(2,1)}), bf16[8,8,2048]{2,1,0:T(8,128)(2,1)S(1)}, u32[]{:S(2)}, u32[]{:S(2)}) async-start(bf16[8,8,2048]{2,1,0:T(8,128)(2,1)} %get-tuple-element.6), calls=%async_computation.3 | async-start | bytes 524288 | tf_op jit(solution)/shard_map/all_to_all | solution.py:148
  250.1 9.5 %all-to-all-done.2 = bf16[8,8,2048]{2,1,0:T(8,128)(2,1)S(1)} async-done(((bf16[8,8,2048]{2,1,0:T(8,128)(2,1)}), bf16[8,8,2048]{2,1,0:T(8,128)(2,1)S(1)}, u32[]{:S(2)}, u32[]{:S(2)}) %all-to-all-start.2) | async-done | bytes 262176 | tf_op jit(solution)/shard_map/all_to_all | solution.py:148
  (86 shorter events, 6.2 us)
Async XLA Ops:
  6.5 150.7 %copy-start = (bf16[1,512,2048]{2,1,0:T(8,128)(2,1)S(1)}, bf16[1,512,2048]{2,1,0:T(8,128)(2,1)}, u32[]{:S(2)}) copy-start(bf16[1,512,2048]{2,1,0:T(8,128)(2,1)} %param.45) | copy-start | bytes 6291460
  6.5 17.3 %copy-start.10 = (s32[16]{0:T(128)S(1)}, s32[16]{0:T(128)}, u32[]{:S(2)}) copy-start(s32[16]{0:T(128)} %param.33) | copy-start | bytes 196
  6.5 17.4 %copy-start.3 = (f32[16,4,384]{2,1,0:T(4,128)S(1)}, f32[16,4,384]{2,1,0:T(4,128)}, u32[]{:S(2)}) copy-start(f32[16,4,384]{2,1,0:T(4,128)} %param.32) | copy-start | bytes 294916
  6.5 17.6 %copy-start.13 = (bf16[2048,4]{0,1:T(4,128)(2,1)S(1)}, bf16[2048,4]{0,1:T(4,128)(2,1)}, u32[]{:S(2)}) copy-start(bf16[2048,4]{0,1:T(4,128)(2,1)} %param.28) | copy-start | bytes 49156
  6.5 17.6 %copy-start.14 = (f32[4]{0:T(128)S(1)}, f32[4]{0:T(128)}, u32[]{:S(2)}) copy-start(f32[4]{0:T(128)} %param.29) | copy-start | bytes 52
  6.5 47.1 %reduce-scatter.3.cloned.1.call-start = ((), (), s32[]{:S(2)}) async-start(), calls=%async_computation.6 | async-start | bytes 884736 | tf_op jit(solution)/shard_map/reduce_scatter | solution.py:89
  23.0 61.2 %all-gather.3.cloned.1.call-start = ((), (), s32[]{:S(2)}) async-start(), calls=%async_computation.7 | async-start | bytes 2359296 | tf_op jit(solution)/shard_map/all_gather | solution.py:105
  23.8 104.6 %all-reduce.4.cloned.1.call-start = ((), (), s32[]{:S(2)}) async-start(), calls=%async_computation.8 | async-start | bytes 262144 | tf_op jit(solution)/shard_map/psum | solution.py:106
  54.7 5.8 %copy-start.1 = (bf16[16,4,384,128]{3,2,1,0:T(8,128)(2,1)S(1)}, bf16[16,4,384,128]{3,2,1,0:T(8,128)(2,1)}, u32[]{:S(2)}) copy-start(bf16[16,4,384,128]{3,2,1,0:T(8,128)(2,1)} %param.31) | copy-start | bytes 18874372
  61.7 66.7 %copy-start.2 = (bf16[16,2048]{1,0:T(8,128)(2,1)S(1)}, bf16[16,2048]{1,0:T(8,128)(2,1)}, u32[]{:S(2)}) copy-start(bf16[16,2048]{1,0:T(8,128)(2,1)} %param.23) | copy-start | bytes 196612
  61.7 67.7 %copy-start.5 = (f32[2048]{0:T(1024)S(1)}, f32[2048]{0:T(1024)}, u32[]{:S(2)}) copy-start(f32[2048]{0:T(1024)} %param.35) | copy-start | bytes 24580
  61.7 78.2 %copy-start.11 = (bf16[256,512]{1,0:T(8,128)(2,1)S(1)}, bf16[256,512]{1,0:T(8,128)(2,1)}, u32[]{:S(2)}) copy-start(bf16[256,512]{1,0:T(8,128)(2,1)} %param.37) | copy-start | bytes 786436
  61.7 78.1 %copy-start.12 = (bf16[256,512]{1,0:T(8,128)(2,1)S(1)}, bf16[256,512]{1,0:T(8,128)(2,1)}, u32[]{:S(2)}) copy-start(bf16[256,512]{1,0:T(8,128)(2,1)} %param.36) | copy-start | bytes 786436
  84.2 57.2 %copy-start.7 = (s32[16,2]{0,1:T(2,128)S(1)}, s32[16,2]{0,1:T(2,128)}, u32[]{:S(2)}) copy-start(s32[16,2]{0,1:T(2,128)} %param.40) | copy-start | bytes 388
  86.9 82.7 %reduce-scatter.5.cloned.1.call-start = ((), (), s32[]{:S(2)}) async-start(), calls=%async_computation.9 | async-start | bytes 294912 | tf_op jit(solution)/shard_map/reduce_scatter | solution.py:112
  140.8 58.9 %all-gather.5.cloned.1.call-start = ((), (), s32[]{:S(2)}) async-start(), calls=%async_computation.10 | async-start | bytes 2359296 | tf_op jit(solution)/shard_map/all_gather | solution.py:121
  141.4 103.8 %all-reduce.6.cloned.1.call-start = ((), (), s32[]{:S(2)}) async-start(), calls=%async_computation.11 | async-start | bytes 655360 | tf_op jit(solution)/shard_map/psum | solution.py:123
  160.4 41.9 %copy-start.8 = (f32[16,2]{0,1:T(2,128)S(1)}, f32[16,2]{0,1:T(2,128)}, u32[]{:S(2)}) copy-start(f32[16,2]{0,1:T(2,128)} %param.42) | copy-start | bytes 388
  160.4 41.9 %copy-start.9 = (f32[16]{0:T(128)S(1)}, f32[16]{0:T(128)}, u32[]{:S(2)}) copy-start(f32[16]{0:T(128)} %param.41) | copy-start | bytes 196
  160.4 89.5 %copy-start.6 = (bf16[2048]{0:T(1024)(128)(2,1)S(1)}, bf16[2048]{0:T(1024)(128)(2,1)}, u32[]{:S(2)}) copy-start(bf16[2048]{0:T(1024)(128)(2,1)} %param.39) | copy-start | bytes 12292
  245.2 15.7 %copy-start.4 = (bf16[16,2048]{1,0:T(8,128)(2,1)S(1)}, bf16[16,2048]{1,0:T(8,128)(2,1)}, u32[]{:S(2)}) copy-start(bf16[16,2048]{1,0:T(8,128)(2,1)} %get-tuple-element.5) | copy-start | bytes 196612
  245.2 14.4 %all-to-all-start.2 = ((bf16[8,8,2048]{2,1,0:T(8,128)(2,1)}), bf16[8,8,2048]{2,1,0:T(8,128)(2,1)S(1)}, u32[]{:S(2)}, u32[]{:S(2)}) async-start(bf16[8,8,2048]{2,1,0:T(8,128)(2,1)} %get-tuple-element.6), calls=%async_computation.3 | async-start | bytes 524288 | tf_op jit(solution)/shard_map/all_to_all | solution.py:148
Sparse Core Ops, SparseCore 0:
  23.2 30.4 reduce-scatter.2
  55.2 28.9 all-gather.2
  87.1 41.2 all-reduce.3
  140.9 28.6 reduce-scatter.4
  171.0 28.6 all-gather.4
  202.5 42.6 all-reduce.5
where the time goes:
time: 269 us; the launch traced here: 268 us
  waiting for transfers between devices  185 us (69%)
  blocking collectives  35.1 us (13%)
  matrix products  20.7 us (8%)
  between operations  13.8 us (5%)
  other arithmetic  6.95 us (3%)
  starting transfers between devices  4.98 us (2%)
    psum x1, waiting for transfers between devices, shards(): lax.psum(dense_terms.astype(jnp.bfloat16), 'tp').astype(jnp.float32)  42.8 us
    psum x1, waiting for transfers between devices, shards(): mixed_heads = lax.psum(head_terms, 'tp')  41.4 us
    all_gather x1, waiting for transfers between devices, shards(): lax.all_gather(dense_down_proj, 'ep', axis=1, tiled=True)  29.4 us
    reduce_scatter x1, waiting for transfers between devices, shards(): lax.psum_scatter(row_term(spread, joined), 'ep', scatter_dimension=0, til...  29.2 us
    all_gather x1, waiting for transfers between devices, shards(): lax.all_gather(output_weight, 'ep', axis=1, tiled=True)  22.4 us
    all_to_all x1, blocking collectives, shards(): lax.all_to_all(outbound, 'ep', split_axis=0, concat_axis=0, tiled=True)  12.7 us
    all_to_all x1, blocking collectives, shards(): lax.all_to_all(normed, 'ep', split_axis=1, concat_axis=0, tiled=True)  12.1 us
    all_to_all x1, blocking collectives, shards(): lax.all_to_all(ffn_in, 'ep', split_axis=1, concat_axis=0, tiled=True)  10.3 us
  transfers between devices with their start and end apart: 7, of which 7 were waited for; matrix products, arithmetic and copies ran while one was open for 6% of the time, Pallas kernels for 0%

commit v1 on v0

--- a/solution.py
+++ b/solution.py
@@ -103,7 +103,21 @@
     )
     attended = attended.reshape(seq_count, head_count * head_size)
     head_terms = right_product(attended, lax.all_gather(output_weight, "ep", axis=1, tiled=True))
-    mixed_heads = lax.psum(head_terms, "tp")
+
+    def _pair_pairs_all(buf):
+        shard_axis = "tp"
+        wide_n = lax.axis_size(shard_axis)
+        next_value, item_now = (buf, 0)
+        while 1 << item_now < wide_n:
+            sheets = []
+            for m in range(wide_n):
+                sheets.append((m, m ^ 1 << item_now))
+            state_now = lax.ppermute(next_value, shard_axis, sheets)
+            next_value = next_value + state_now
+            item_now = item_now + 1
+        return next_value
+
+    mixed_heads = _pair_pairs_all(head_terms)
     residual = (tokens.astype(jnp.float32) + mixed_heads).astype(jnp.bfloat16)
     ffn_in = rms_scale(residual, ffn_gain).astype(jnp.bfloat16)
     dense_width = dense_gate_proj.shape[1]

time: 269 us -> 236 us (0.88)
  waiting for transfers between devices: 185 us -> 150 us
  starting transfers between devices: 4.98 us -> 7.81 us
    psum x1 -> x0, waiting for transfers between devices: 41.4 us -> none  [shards(): mixed_heads = lax.psum(head_terms, 'tp')]
    ppermute x0 -> x2, waiting for transfers between devices: none -> 7.8 us  [_pair_pairs_all(): state_now = lax.ppermute(next_value, shard_axis, sheets)]
    ppermute x0 -> x2, starting transfers between devices: none -> 2.87 us  [_pair_pairs_all(): state_now = lax.ppermute(next_value, shard_axis, sheets)]
  transfers between devices with their start and end apart: 7 -> 8, of which waited for: 7 -> 8; matrix products, arithmetic and copies ran while one was open for 6% -> 7% of each run, Pallas kernels for 0% -> 0%
where the time goes in v1:
time: 236 us; the launch traced here: 235 us
  waiting for transfers between devices  150 us (64%)
  blocking collectives  35.2 us (15%)
  matrix products  20 us (8%)
  between operations  13.4 us (6%)
  starting transfers between devices  7.81 us (3%)
  other arithmetic  6.07 us (3%)
    psum x1, waiting for transfers between devices, shards(): lax.psum(dense_terms.astype(jnp.bfloat16), 'tp').astype(jnp.float32)  42.8 us
    all_gather x1, waiting for transfers between devices, shards(): lax.all_gather(dense_down_proj, 'ep', axis=1, tiled=True)  29.5 us
    reduce_scatter x1, waiting for transfers between devices, shards(): lax.psum_scatter(row_term(spread, joined), 'ep', scatter_dimension=0, til...  29.2 us
    all_gather x1, waiting for transfers between devices, shards(): lax.all_gather(output_weight, 'ep', axis=1, tiled=True)  22.4 us
    all_to_all x1, blocking collectives, shards(): lax.all_to_all(outbound, 'ep', split_axis=0, concat_axis=0, tiled=True)  12.9 us
    all_to_all x1, blocking collectives, shards(): lax.all_to_all(normed, 'ep', split_axis=1, concat_axis=0, tiled=True)  12.1 us
    all_to_all x1, blocking collectives, shards(): lax.all_to_all(ffn_in, 'ep', split_axis=1, concat_axis=0, tiled=True)  10.2 us
    all_to_all x1, waiting for transfers between devices, shards(): lax.all_to_all(expert_result.reshape(sources, slots_now, feature).astype(...  9.53 us
  transfers between devices with their start and end apart: 8, of which 8 were waited for; matrix products, arithmetic and copies ran while one was open for 7% of the time, Pallas kernels for 0%

profile of v1, /device:TPU:0, one launch (start us, length us, event | category | flops | bytes accessed | tf_op | source)
XLA Modules:
  0.0 234.9 jit_solution(17800277466005070437)
XLA Ops:
  6.6 1.1 fusion.32
  7.7 0.9 fusion.34
  8.7 12.1 %all_to_all.48 = bf16[16,8,256]{2,0,1:T(8,128)(2,1)S(1)} all-to-all(bf16[16,8,256]{2,0,1:T(8,128)(2,1)S(1)} %bitcast.96), channel_id=1, replica_groups=mesh['ep'=8,'tp'=4] {'ep'}, dimensions={1} | all-to-all | bytes 131072 | tf_op jit(solution)/shard_map/all_to_all | solution.py:87
  20.7 2.3 fusion.20
  24.4 29.2 %reduce-scatter.3.cloned.1.call-done = f32[16,1536]{1,0:T(8,128)} async-done(((f32[128,1536]{1,0:T(8,128)}), f32[16,1536]{1,0:T(8,128)}) %reduce-scatter.3.cloned.1.call-update) | async-done | bytes 98320 | tf_op jit(solution)/shard_map/reduce_scatter | solution.py:89
  54.7 5.2 %fusion.80 = f32[16,4,1,384]{3,2,1,0:T(1,128)S(1)} fusion(bf16[16,4,128,1]{2,3,1,0:T(2,128)(2,1)S(1)} %reshape.151, bf16[16,4,384,128]{3,2,1,0:T(8,128)(2,1)} %param.30), kind=kOutput, calls=%fused_computation.117 | convolution fusion | flops 6291456 | bytes 6406144 | tf_op jit(solution)/shard_map/shd,shpd->shp/dot_general | solution.py:28
  60.5 1.2 fusion.48
  61.8 22.4 %all-gather.3.cloned.1.call-done = bf16[512,2048]{1,0:T(8,128)(2,1)} async-done(((bf16[512,256]{1,0:T(8,128)(2,1)}), bf16[512,2048]{1,0:T(8,128)(2,1)}) %all-gather.3.cloned.1.call-update) | async-done | bytes 2097168 | tf_op jit(solution)/shard_map/all_gather | solution.py:105
  84.2 2.0 fusion.55
  86.2 1.4 collective-permute-start
  87.6 4.2 %collective-permute-done = f32[16,2048]{1,0:T(8,128)S(1)} collective-permute-done((f32[16,2048]{1,0:T(8,128)S(1)}, f32[16,2048]{1,0:T(8,128)S(1)}, u32[]{:S(2)}, u32[]{:S(2)}) %collective-permute-start) | collective-permute-done | bytes 131104 | tf_op jit(solution)/shard_map/ppermute | solution.py:115
  91.8 1.5 collective-permute-start.1
  93.3 3.6 %collective-permute-done.1 = f32[16,2048]{1,0:T(8,128)S(1)} collective-permute-done((f32[16,2048]{1,0:T(8,128)S(1)}, f32[16,2048]{1,0:T(8,128)S(1)}, u32[]{:S(2)}, u32[]{:S(2)}) %collective-permute-start.1) | collective-permute-done | bytes 131104 | tf_op jit(solution)/shard_map/ppermute | solution.py:115
  97.1 10.2 %all_to_all.49 = bf16[16,8,256]{2,0,1:T(8,128)(2,1)S(1)} all-to-all(bf16[16,8,256]{2,0,1:T(8,128)(2,1)S(1)} %bitcast.97), channel_id=1, replica_groups=mesh['ep'=8,'tp'=4] {'ep'}, dimensions={1} | all-to-all | bytes 131072 | tf_op jit(solution)/shard_map/all_to_all | solution.py:124
  107.4 0.9 convolution_convert_fusion.3
  110.0 12.9 %all_to_all.50 = bf16[8,8,2048]{2,1,0:T(8,128)(2,1)S(1)} all-to-all(bf16[8,8,2048]{2,1,0:T(8,128)(2,1)S(1)} %fusion), channel_id=1, replica_groups=mesh['ep'=8,'tp'=4] {'ep'}, dimensions={0} | all-to-all | bytes 524288 | tf_op jit(solution)/shard_map/all_to_all | solution.py:154
  122.9 2.1 fusion.5
  125.0 3.2 %fusion.1 = bf16[8,8,2048]{2,1,0:T(8,128)(2,1)} fusion(bf16[1,512,2048]{2,1,0:T(8,128)(2,1)S(1)} %copy-done, bf16[1,2048,512]{2,1,0:T(8,128)(2,1)} %param.44, bf16[8,8,2048]{2,1,0:T(8,128)(2,1)S(1)} %all_to_all.50, f32[64,512]{1,0:T(8,128)S(1)} %fusion.5), kind=kOutput, calls=%fused_computation.5 | convolution fusion | flops 268763136 | bytes 4849664 | tf_op jit(solution)/shard_map/dot_general | solution.py:160
  128.2 8.0 %reduce-scatter.5.cloned.1.call-done = bf16[16,1024]{1,0:T(8,128)(2,1)} async-done(((bf16[128,1024]{1,0:T(8,128)(2,1)}), bf16[16,1024]{1,0:T(8,128)(2,1)}) %reduce-scatter.5.cloned.1.call-update) | async-done | bytes 32784 | tf_op jit(solution)/shard_map/reduce_scatter | solution.py:126
  136.9 29.5 %all-gather.5.cloned.1.call-done = bf16[512,2048]{1,0:T(8,128)(2,1)} async-done(((bf16[512,256]{1,0:T(8,128)(2,1)}), bf16[512,2048]{1,0:T(8,128)(2,1)}) %all-gather.5.cloned.1.call-update) | async-done | bytes 2097168 | tf_op jit(solution)/shard_map/all_gather | solution.py:135
  166.4 2.6 %convolution_convert_fusion.2 = bf16[16,2048]{1,0:T(8,128)(2,1)} fusion(bf16[512,2048]{1,0:T(8,128)(2,1)} %all-gather.5.cloned.1.call-done, f32[16,1024]{1,0:T(8,128)S(1)} %convert_element_type.119), kind=kOutput, calls=%fused_computation.6 | convolution fusion | flops 33636352 | bytes 2228224 | tf_op jit(solution)/shard_map/dot_general | solution.py:54
  169.1 42.8 %all-reduce.3.cloned.1.call-done = (bf16[16,2048]{1,0:T(8,128)(2,1)}, bf16[8,8,2048]{2,1,0:T(8,128)(2,1)}) async-done(((bf16[16,2048]{1,0:T(8,128)(2,1)}, bf16[8,8,2048]{2,1,0:T(8,128)(2,1)}), (bf16[16,2048]{1,0:T(8,128)(2,1)}, bf16[8,8,2048]{2,1,0:T(8,128)(2,1)})) %all-reduce.3.cloned.1.call-update) | async-done | bytes 327696 | tf_op jit(solution)/shard_map/psum | solution.py:137
  211.9 4.7 %all-to-all-start.2 = ((bf16[8,8,2048]{2,1,0:T(8,128)(2,1)}), bf16[8,8,2048]{2,1,0:T(8,128)(2,1)S(1)}, u32[]{:S(2)}, u32[]{:S(2)}) async-start(bf16[8,8,2048]{2,1,0:T(8,128)(2,1)} %get-tuple-element.6), calls=%async_computation.3 | async-start | bytes 524288 | tf_op jit(solution)/shard_map/all_to_all | solution.py:162
  216.8 9.5 %all-to-all-done.2 = bf16[8,8,2048]{2,1,0:T(8,128)(2,1)S(1)} async-done(((bf16[8,8,2048]{2,1,0:T(8,128)(2,1)}), bf16[8,8,2048]{2,1,0:T(8,128)(2,1)S(1)}, u32[]{:S(2)}, u32[]{:S(2)}) %all-to-all-start.2) | async-done | bytes 262176 | tf_op jit(solution)/shard_map/all_to_all | solution.py:162
  (88 shorter events, 8.0 us)
Async XLA Ops:
  6.5 118.4 %copy-start = (bf16[1,512,2048]{2,1,0:T(8,128)(2,1)S(1)}, bf16[1,512,2048]{2,1,0:T(8,128)(2,1)}, u32[]{:S(2)}) copy-start(bf16[1,512,2048]{2,1,0:T(8,128)(2,1)} %param.45) | copy-start | bytes 6291460
  6.5 17.3 %copy-start.10 = (s32[16]{0:T(128)S(1)}, s32[16]{0:T(128)}, u32[]{:S(2)}) copy-start(s32[16]{0:T(128)} %param.33) | copy-start | bytes 196
  6.5 17.4 %copy-start.3 = (f32[16,4,384]{2,1,0:T(4,128)S(1)}, f32[16,4,384]{2,1,0:T(4,128)}, u32[]{:S(2)}) copy-start(f32[16,4,384]{2,1,0:T(4,128)} %param.32) | copy-start | bytes 294916
  6.5 17.6 %copy-start.13 = (bf16[2048,4]{0,1:T(4,128)(2,1)S(1)}, bf16[2048,4]{0,1:T(4,128)(2,1)}, u32[]{:S(2)}) copy-start(bf16[2048,4]{0,1:T(4,128)(2,1)} %param.28) | copy-start | bytes 49156
  6.5 17.6 %copy-start.14 = (f32[4]{0:T(128)S(1)}, f32[4]{0:T(128)}, u32[]{:S(2)}) copy-start(f32[4]{0:T(128)} %param.29) | copy-start | bytes 52
  6.5 47.1 %reduce-scatter.3.cloned.1.call-start = ((), (), s32[]{:S(2)}) async-start(), calls=%async_computation.6 | async-start | bytes 884736 | tf_op jit(solution)/shard_map/reduce_scatter | solution.py:89
  23.0 61.2 %all-gather.3.cloned.1.call-start = ((), (), s32[]{:S(2)}) async-start(), calls=%async_computation.7 | async-start | bytes 2359296 | tf_op jit(solution)/shard_map/all_gather | solution.py:105
  23.8 112.4 %reduce-scatter.5.cloned.1.call-start = ((), (), s32[]{:S(2)}) async-start(), calls=%async_computation.8 | async-start | bytes 294912 | tf_op jit(solution)/shard_map/reduce_scatter | solution.py:126
  54.7 5.8 %copy-start.1 = (bf16[16,4,384,128]{3,2,1,0:T(8,128)(2,1)S(1)}, bf16[16,4,384,128]{3,2,1,0:T(8,128)(2,1)}, u32[]{:S(2)}) copy-start(bf16[16,4,384,128]{3,2,1,0:T(8,128)(2,1)} %param.31) | copy-start | bytes 18874372
  61.6 35.2 %copy-start.2 = (bf16[16,2048]{1,0:T(8,128)(2,1)S(1)}, bf16[16,2048]{1,0:T(8,128)(2,1)}, u32[]{:S(2)}) copy-start(bf16[16,2048]{1,0:T(8,128)(2,1)} %param.23) | copy-start | bytes 196612
  61.6 35.4 %copy-start.5 = (f32[2048]{0:T(1024)S(1)}, f32[2048]{0:T(1024)}, u32[]{:S(2)}) copy-start(f32[2048]{0:T(1024)} %param.35) | copy-start | bytes 24580
  61.6 45.7 %copy-start.11 = (bf16[256,512]{1,0:T(8,128)(2,1)S(1)}, bf16[256,512]{1,0:T(8,128)(2,1)}, u32[]{:S(2)}) copy-start(bf16[256,512]{1,0:T(8,128)(2,1)} %param.37) | copy-start | bytes 786436
  61.7 45.7 %copy-start.12 = (bf16[256,512]{1,0:T(8,128)(2,1)S(1)}, bf16[256,512]{1,0:T(8,128)(2,1)}, u32[]{:S(2)}) copy-start(bf16[256,512]{1,0:T(8,128)(2,1)} %param.36) | copy-start | bytes 786436
  84.2 24.8 %copy-start.7 = (s32[16,2]{0,1:T(2,128)S(1)}, s32[16,2]{0,1:T(2,128)}, u32[]{:S(2)}) copy-start(s32[16,2]{0,1:T(2,128)} %param.40) | copy-start | bytes 388
  86.2 5.6 %collective-permute-start = (f32[16,2048]{1,0:T(8,128)S(1)}, f32[16,2048]{1,0:T(8,128)S(1)}, u32[]{:S(2)}, u32[]{:S(2)}) collective-permute-start(f32[16,2048]{1,0:T(8,128)S(1)} %fusion.55), channel_id=1, source_target_pairs={{0,1},{1,0},{2,3},{3,2},{4,5},{5,4},{6,7},{7,6},{8,9},{9,8},{10,11... | collective-permute-start | bytes 393224 | tf_op jit(solution)/shard_map/ppermute | solution.py:115
  91.8 5.0 %collective-permute-start.1 = (f32[16,2048]{1,0:T(8,128)S(1)}, f32[16,2048]{1,0:T(8,128)S(1)}, u32[]{:S(2)}, u32[]{:S(2)}) collective-permute-start(f32[16,2048]{1,0:T(8,128)S(1)} %add.116), channel_id=1, source_target_pairs={{0,2},{1,3},{2,0},{3,1},{4,6},{5,7},{6,4},{7,5},{8,10},{9,11},{10,... | collective-permute-start | bytes 393224 | tf_op jit(solution)/shard_map/ppermute | solution.py:115
  108.3 58.1 %all-gather.5.cloned.1.call-start = ((), (), s32[]{:S(2)}) async-start(), calls=%async_computation.9 | async-start | bytes 2359296 | tf_op jit(solution)/shard_map/all_gather | solution.py:135
  108.9 103.0 %all-reduce.3.cloned.1.call-start = ((), (), s32[]{:S(2)}) async-start(), calls=%async_computation.10 | async-start | bytes 655360 | tf_op jit(solution)/shard_map/psum | solution.py:137
  128.2 40.9 %copy-start.8 = (f32[16,2]{0,1:T(2,128)S(1)}, f32[16,2]{0,1:T(2,128)}, u32[]{:S(2)}) copy-start(f32[16,2]{0,1:T(2,128)} %param.42) | copy-start | bytes 388
  128.2 40.9 %copy-start.9 = (f32[16]{0:T(128)S(1)}, f32[16]{0:T(128)}, u32[]{:S(2)}) copy-start(f32[16]{0:T(128)} %param.41) | copy-start | bytes 196
  128.2 88.5 %copy-start.6 = (bf16[2048]{0:T(1024)(128)(2,1)S(1)}, bf16[2048]{0:T(1024)(128)(2,1)}, u32[]{:S(2)}) copy-start(bf16[2048]{0:T(1024)(128)(2,1)} %param.39) | copy-start | bytes 12292
  211.9 15.7 %copy-start.4 = (bf16[16,2048]{1,0:T(8,128)(2,1)S(1)}, bf16[16,2048]{1,0:T(8,128)(2,1)}, u32[]{:S(2)}) copy-start(bf16[16,2048]{1,0:T(8,128)(2,1)} %get-tuple-element.5) | copy-start | bytes 196612
  211.9 14.4 %all-to-all-start.2 = ((bf16[8,8,2048]{2,1,0:T(8,128)(2,1)}), bf16[8,8,2048]{2,1,0:T(8,128)(2,1)S(1)}, u32[]{:S(2)}, u32[]{:S(2)}) async-start(bf16[8,8,2048]{2,1,0:T(8,128)(2,1)} %get-tuple-element.6), calls=%async_computation.3 | async-start | bytes 524288 | tf_op jit(solution)/shard_map/all_to_all | solution.py:162
Sparse Core Ops, SparseCore 0:
  23.1 30.4 reduce-scatter.2
  55.2 28.9 all-gather.2
  108.4 27.6 reduce-scatter.4
  137.6 28.7 all-gather.4
  169.2 42.6 all-reduce.2
